TPU v7x, 256 devices: a whole 4x4x8 slice. The times are simulated.
256 devices in a mesh: gr: 2 (over z_hi), fs: 16 (over z_lo, x), tp: 8 (over y, core).
Axes of the slice: x: 4, y: 4, z: 8 (z_hi: 2, z_lo: 4; z = z_hi * 4 + z_lo), core: 2. Of those that a mesh axis runs over, the one named last changes fastest.
Arguments:
- tokens: bfloat16 [6144, 4096], P(('gr', 'fs'), 'tp'), may hold values from -6 to 6
- route_ids: int32 [6144, 2], P(('gr', 'fs')), may hold values from 0 to 15, all different within a row; in each aligned block of 192 rows (0 to 191, 192 to 383, ...) at most 48 rows name the same one
- route_logits: float32 [6144, 2], P(('gr', 'fs')), may hold values from -6 to 6
- gain: float32 [4096], P(('gr', 'fs')), may hold values from 0.1 to 1.9
- gate_master: float32 [16, 4096, 2048], P(None, ('gr', 'fs'), 'tp'), may hold values from -6 to 6
- up_master: float32 [16, 4096, 2048], P(None, ('gr', 'fs'), 'tp'), may hold values from -6 to 6
- down_master: float32 [16, 2048, 4096], P(None, ('gr', 'fs'), 'tp'), may hold values from -6 to 6
Outputs:
- gate_weight: bfloat16 [16, 4096, 2048], P('fs', None, 'tp')
- up_weight: bfloat16 [16, 4096, 2048], P('fs', None, 'tp')
- down_weight: bfloat16 [16, 2048, 4096], P('fs', 'tp')
- mixed_out: bfloat16 [6144, 4096], P(('gr', 'fs'), 'tp')
Inputs may be any that keep to these rules, and one draw needn't show every extreme that they name: `route_ids`: each row names 2 different experts; among the rows of one device no expert is named by more than 48 rows, a bound that some block reaches.
All inputs are finite; a program needn't handle non-finite values.
Results may differ from a plain program's by a relative error of at most 0.015.
Values may be sent and summed in bfloat16 or wider, within the bound.
A program may use at most 128 MiB of HBM per device.

v0:
```python
import jax
import jax.numpy as jnp
from jax import lax
from jax.sharding import PartitionSpec as P

EPS = 1e-06


def from_everyone(array, axis):
    copies = jnp.broadcast_to(array, (lax.axis_size(axis), *array.shape))
    return lax.all_to_all(copies, axis, split_axis=0, concat_axis=0, tiled=True)


def of_everyone(array, axis):
    return from_everyone(array, axis).sum(axis=0)


def slot_tables(route_ids, experts, capacity):
    assign_count = route_ids.shape[0] * route_ids.shape[1]
    flattened = route_ids.reshape(assign_count)
    onehot = (flattened[:, None] == jnp.arange(experts, dtype=jnp.int32)[None, :]).astype(jnp.int32)
    earlier = jnp.cumsum(onehot, axis=0) - onehot
    slot_rank = jnp.sum(earlier * onehot, axis=1)
    position = flattened * capacity + slot_rank
    source = (
        jnp.full((experts * capacity,), assign_count, jnp.int32)
        .at[position]
        .set(jnp.arange(assign_count, dtype=jnp.int32))
    )
    return (position, source)


def fill_slots(normed, source, top_count, experts, capacity):
    token_total = normed.shape[0]
    padded = jnp.concatenate([normed, jnp.zeros((1, normed.shape[1]), normed.dtype)], axis=0)
    token_index = jnp.where(source < token_total * top_count, source // top_count, token_total)
    return padded[token_index].reshape(experts, capacity, normed.shape[1])


def body(tokens, route_ids, route_logits, gain, gate_master, up_master, down_master):
    experts = gate_master.shape[0]
    token_total = route_ids.shape[0]
    top_count = route_ids.shape[1]
    capacity = 2 * token_total * top_count // experts
    row_gain = gain[None, :, None]
    gate_cast = (gate_master * row_gain).astype(jnp.bfloat16)
    up_cast = (up_master * row_gain).astype(jnp.bfloat16)
    down_cast = down_master.astype(jnp.bfloat16)
    copies = lax.axis_size("gr")
    gate_full, up_full, down_full = (
        lax.all_to_all(
            jnp.tile(gate_cast, (copies, 1, 1)),
            ("gr", "fs"),
            split_axis=0,
            concat_axis=1,
            tiled=True,
        ),
        lax.all_to_all(
            jnp.tile(up_cast, (copies, 1, 1)), ("gr", "fs"), split_axis=0, concat_axis=1, tiled=True
        ),
        lax.all_to_all(
            jnp.tile(down_cast, (copies, 1, 1)),
            ("gr", "fs"),
            split_axis=0,
            concat_axis=1,
            tiled=True,
        ),
    )
    down_rows = lax.all_to_all(down_full, "tp", split_axis=1, concat_axis=2, tiled=True)
    sigmoid_vals = jax.nn.sigmoid(route_logits)
    shares = sigmoid_vals / jnp.sum(sigmoid_vals, axis=1, keepdims=True)
    position, source = slot_tables(route_ids, experts, capacity)
    model_width = gate_full.shape[1]
    float_rows = tokens.astype(jnp.float32)
    squares = of_everyone(jnp.sum(float_rows * float_rows, axis=1), "tp")
    normed = (float_rows * lax.rsqrt(squares[:, None] / model_width + EPS)).astype(jnp.bfloat16)
    buffer = fill_slots(normed, source, top_count, experts, capacity)
    arrived = lax.all_to_all(buffer, "fs", split_axis=0, concat_axis=1, tiled=True)
    block_rows = lax.all_gather(arrived, "tp", axis=2, tiled=True)
    gate_sum = jnp.einsum("erd,edf->erf", block_rows, gate_full, preferred_element_type=jnp.float32)
    up_sum = jnp.einsum("erd,edf->erf", block_rows, up_full, preferred_element_type=jnp.float32)
    scale_in = model_width ** (-0.5)
    hidden = (jax.nn.silu(gate_sum * scale_in) * (up_sum * scale_in)).astype(jnp.bfloat16)
    partial_value = jnp.einsum(
        "erf,efd->erd", hidden, down_rows, preferred_element_type=jnp.float32
    )
    summed = lax.psum_scatter(
        partial_value.astype(jnp.bfloat16), "tp", scatter_dimension=2, tiled=True
    ).astype(jnp.float32)
    expert_out = (summed * down_full.shape[1] ** (-0.5)).astype(jnp.bfloat16)
    returned = lax.all_to_all(expert_out, "fs", split_axis=1, concat_axis=0, tiled=True)
    picked = returned.reshape(experts * capacity, returned.shape[2])[position].astype(jnp.float32)
    weighted = picked * shares.reshape(token_total * top_count)[:, None]
    mixed_out = jnp.sum(weighted.reshape(token_total, top_count, returned.shape[2]), axis=1).astype(
        jnp.bfloat16
    )
    return (gate_full, up_full, down_rows, mixed_out)


def solution(mesh):
    in_specs = (
        P(("gr", "fs"), "tp"),
        P(("gr", "fs"), None),
        P(("gr", "fs"), None),
        P(("gr", "fs")),
        P(None, ("gr", "fs"), "tp"),
        P(None, ("gr", "fs"), "tp"),
        P(None, ("gr", "fs"), "tp"),
    )
    out_specs = (
        P("fs", None, "tp"),
        P("fs", None, "tp"),
        P("fs", "tp", None),
        P(("gr", "fs"), "tp"),
    )
    return jax.shard_map(body, mesh=mesh, in_specs=in_specs, out_specs=out_specs, check_vma=False)
```

profile of v0, /device:TPU:32, one launch (start us, length us, event | category | flops | bytes accessed | tf_op | source)
XLA Modules:
  0.0 369.7 jit_solution(7977077807595806848)
XLA Ops:
  7.2 1.0 fusion.19
  8.2 0.6 broadcast_in_dim.7
  8.8 4.5 %all-to-all-start.4 = ((f32[8,1,192]{2,1,0:T(1,128)}), f32[8,1,192]{2,1,0:T(1,128)S(1)}, u32[]{:S(2)}, u32[]{:S(2)}) async-start(f32[8,1,192]{2,1,0:T(1,128)} %broadcast_in_dim.7), calls=%async_computation.4 | async-start | bytes 16384 | tf_op jit(solution)/shard_map/all_to_all | solution.py:11
  13.3 0.8 copy.58
  14.4 0.7 broadcast_multiply_fusion
  15.1 0.9 reduce-window.6
  15.9 0.2 slice_reduce_fusion
  16.6 2.9 scatter_custom_fusion
  19.6 1.0 fusion.20
  20.7 3.3 gather_fusion
  24.0 8.5 %all-to-all-start.5 = ((bf16[16,48,512]{2,1,0:T(8,128)(2,1)}), bf16[16,48,512]{2,1,0:T(8,128)(2,1)S(1)}, u32[]{:S(2)}, u32[]{:S(2)}) async-start(bf16[16,48,512]{2,1,0:T(8,128)(2,1)} %bitcast.9), calls=%async_computation.5 | async-start | bytes 1572864 | tf_op jit(solution)/shard_map/all_to_all | solution.py:78
  32.5 1.7 convert_element_type.50
  34.2 19.2 %all-to-all-done.5 = bf16[16,48,512]{2,1,0:T(8,128)(2,1)S(1)} async-done(((bf16[16,48,512]{2,1,0:T(8,128)(2,1)}), bf16[16,48,512]{2,1,0:T(8,128)(2,1)S(1)}, u32[]{:S(2)}, u32[]{:S(2)}) %all-to-all-start.5) | async-done | bytes 786464 | tf_op jit(solution)/shard_map/all_to_all | solution.py:78
  53.4 1.6 tile.31
  55.0 8.0 %all-to-all-start.2 = ((bf16[32,64,512]{2,1,0:T(8,128)(2,1)}), bf16[32,64,512]{2,1,0:T(8,128)(2,1)S(1)}, u32[]{:S(2)}, u32[]{:S(2)}) async-start(bf16[32,64,512]{2,1,0:T(8,128)(2,1)} %bitcast.73), calls=%async_computation.2 | async-start | bytes 4194304 | tf_op jit(solution)/shard_map/all_to_all | solution.py:61
  63.1 0.7 all-gather.2.cloned.1.call-update
  63.8 3.7 %multiply_convert_fusion = (bf16[16,128,256]{2,1,0:T(8,128)(2,1)S(1)}, bf16[16,128,256]{2,1,0:T(8,128)(2,1)}) fusion(f32[16,128,256]{2,1,0:T(8,128)} %param.12, f32[128]{0:T(128)S(1)} %copy-done.3, f32[16,128,256]{2,1,0:T(8,128)} %param.11), kind=kLoop, calls=%fused_computation.9 | loop fusion | flops 2097152 | bytes 6291968 | tf_op jit(solution)/shard_map/convert_element_type | solution.py:47
  67.5 44.7 %all-to-all-done.2 = bf16[32,64,512]{2,1,0:T(8,128)(2,1)S(1)} async-done(((bf16[32,64,512]{2,1,0:T(8,128)(2,1)}), bf16[32,64,512]{2,1,0:T(8,128)(2,1)S(1)}, u32[]{:S(2)}, u32[]{:S(2)}) %all-to-all-start.2) | async-done | bytes 2097184 | tf_op jit(solution)/shard_map/all_to_all | solution.py:61
  112.2 2.8 tile.12
  115.0 6.5 %all-to-all-start = ((bf16[32,128,256]{2,1,0:T(8,128)(2,1)}), bf16[32,128,256]{2,1,0:T(8,128)(2,1)}, u32[]{:S(2)}, u32[]{:S(2)}) async-start(bf16[32,128,256]{2,1,0:T(8,128)(2,1)} %bitcast.75), calls=%async_computation | async-start | bytes 4194304 | tf_op jit(solution)/shard_map/all_to_all | solution.py:51
  121.5 18.5 %copy.74 = bf16[1,2048,512]{2,0,1:T(2,128)(2,1)} copy(bf16[1,2048,512]{2,1,0:T(8,128)(2,1)S(1)} %bitcast.69) | data formatting | bytes 4194304 | tf_op jit(solution)/shard_map/all_to_all | solution.py:61
  140.1 0.5 broadcast.134
  140.6 14.1 %reduce.5 = bf16[2048,512]{1,0:T(8,128)(2,1)S(1)} reduce(bf16[2048,1,512]{2,1,0:T(2,128)(2,1)} %bitcast.67, bf16[]{:T(256)} %broadcast.134), dimensions={1}, to_apply=%bitcast.63.reduce_sub_computation | reduce | bytes 4194306
  154.7 3.8 %reshape.180 = bf16[8,2,65536]{2,1,0:T(2,128)(2,1)} reshape(bf16[2048,512]{1,0:T(8,128)(2,1)S(1)} %reduce.5) | data formatting | bytes 4194304
  158.4 11.4 %all-to-all-done = bf16[32,128,256]{2,1,0:T(8,128)(2,1)} async-done(((bf16[32,128,256]{2,1,0:T(8,128)(2,1)}), bf16[32,128,256]{2,1,0:T(8,128)(2,1)}, u32[]{:S(2)}, u32[]{:S(2)}) %all-to-all-start) | async-done | bytes 2097184 | tf_op jit(solution)/shard_map/all_to_all | solution.py:51
  169.8 31.4 %all_to_all.81 = bf16[8,2,65536]{2,1,0:T(2,128)(2,1)S(1)} all-to-all(bf16[8,2,65536]{2,1,0:T(2,128)(2,1)} %reshape.180), channel_id=1, replica_groups=mesh['gr'=2,'fs'=16,'tp'=8] {'tp'}, dimensions={0} | all-to-all | bytes 4194304 | tf_op jit(solution)/shard_map/all_to_all | solution.py:69
  201.2 1.6 tile.14
  202.8 6.5 %all-to-all-start.1 = ((bf16[32,128,256]{2,1,0:T(8,128)(2,1)}), bf16[32,128,256]{2,1,0:T(8,128)(2,1)}, u32[]{:S(2)}, u32[]{:S(2)}) async-start(bf16[32,128,256]{2,1,0:T(8,128)(2,1)} %bitcast.74), calls=%async_computation.1 | async-start | bytes 4194304 | tf_op jit(solution)/shard_map/all_to_all | solution.py:58
  209.4 4.5 %reshape.181 = bf16[2048,1,512]{2,1,0:T(2,128)(2,1)} reshape(bf16[8,2,65536]{2,1,0:T(2,128)(2,1)S(1)} %all_to_all.81) | data formatting | bytes 4194304
  213.8 2.8 copy.65
  216.6 2.4 copy.55
  219.0 5.3 %fusion.5 = f32[768,256]{1,0:T(8,128)S(1)} fusion(bf16[4096,256]{1,0:T(8,128)(2,1)} %bitcast.12, bf16[1,768,4096]{2,1,0:T(8,128)(2,1)} %all-gather.2.cloned.1.call-done), kind=kOutput, calls=%fused_computation.12 | convolution fusion | flops 1610809344 | bytes 9175040 | tf_op jit(solution)/shard_map/erd,edf->erf/dot_general | solution.py:80
  224.3 34.3 %all-to-all-done.1 = bf16[32,128,256]{2,1,0:T(8,128)(2,1)} async-done(((bf16[32,128,256]{2,1,0:T(8,128)(2,1)}), bf16[32,128,256]{2,1,0:T(8,128)(2,1)}, u32[]{:S(2)}, u32[]{:S(2)}) %all-to-all-start.1) | async-done | bytes 2097184 | tf_op jit(solution)/shard_map/all_to_all | solution.py:58
  258.6 12.7 %fusion.4 = bf16[1,768,4096]{2,1,0:T(8,128)(2,1)} fusion(bf16[256,4096]{0,1:T(8,128)(2,1)S(1)} %bitcast.71, bf16[4096,256]{1,0:T(8,128)(2,1)} %bitcast.13, bf16[1,768,4096]{2,1,0:T(8,128)(2,1)} %all-gather.2.cloned.1.call-done, f32[768,256]{1,0:T(8,128)S(1)} %fusion.5), kind=kOutput, calls=%fused_computation.8 | convolution fusion | flops 3225747456 | bytes 17563648 | tf_op jit(solution)/shard_map/erf,efd->erd/dot_general | solution.py:84
  271.3 41.1 %reduce-scatter.2.cloned.1.call-done = bf16[1,768,512]{2,1,0:T(8,128)(2,1)} async-done(((bf16[1,768,4096]{2,1,0:T(8,128)(2,1)}), bf16[1,768,512]{2,1,0:T(8,128)(2,1)}) %reduce-scatter.2.cloned.1.call-update) | async-done | bytes 786448 | tf_op jit(solution)/shard_map/reduce_scatter | solution.py:87
  312.4 1.3 multiply_convert_fusion.2
  313.7 2.4 copy.75
  316.0 6.6 %reduce.6 = bf16[768,512]{1,0:T(8,128)(2,1)S(1)} reduce(bf16[768,1,512]{2,1,0:T(2,128)(2,1)} %bitcast.76, bf16[]{:T(256)} %broadcast.134), dimensions={1}, to_apply=%bitcast.64.reduce_sub_computation | reduce | bytes 1572866
  322.7 1.4 reshape.182
  324.1 7.7 %all-to-all-start.6 = ((bf16[16,2,12288]{2,1,0:T(2,128)(2,1)}), bf16[16,2,12288]{2,1,0:T(2,128)(2,1)S(1)}, u32[]{:S(2)}, u32[]{:S(2)}) async-start(bf16[16,2,12288]{2,1,0:T(2,128)(2,1)} %reshape.182), calls=%async_computation.7 | async-start | bytes 1572864 | tf_op jit(solution)/shard_map/all_to_all | solution.py:91
  332.0 2.9 copy.64
  334.9 16.7 %all-to-all-done.6 = bf16[16,2,12288]{2,1,0:T(2,128)(2,1)S(1)} async-done(((bf16[16,2,12288]{2,1,0:T(2,128)(2,1)}), bf16[16,2,12288]{2,1,0:T(2,128)(2,1)S(1)}, u32[]{:S(2)}, u32[]{:S(2)}) %all-to-all-start.6) | async-done | bytes 786464 | tf_op jit(solution)/shard_map/all_to_all | solution.py:91
  351.5 0.7 reshape.183
  352.5 2.1 gather_fusion.1
  354.6 0.5 reshape.150
  355.1 1.7 multiply_reduce_fusion
  356.8 3.0 copy.78
  359.8 3.0 copy.79
  (32 shorter events, 1.3 us)
Async XLA Ops:
  8.8 10.7 %all-to-all-start.4 = ((f32[8,1,192]{2,1,0:T(1,128)}), f32[8,1,192]{2,1,0:T(1,128)S(1)}, u32[]{:S(2)}, u32[]{:S(2)}) async-start(f32[8,1,192]{2,1,0:T(1,128)} %broadcast_in_dim.7), calls=%async_computation.4 | async-start | bytes 16384 | tf_op jit(solution)/shard_map/all_to_all | solution.py:11
  24.0 29.4 %all-to-all-start.5 = ((bf16[16,48,512]{2,1,0:T(8,128)(2,1)}), bf16[16,48,512]{2,1,0:T(8,128)(2,1)S(1)}, u32[]{:S(2)}, u32[]{:S(2)}) async-start(bf16[16,48,512]{2,1,0:T(8,128)(2,1)} %bitcast.9), calls=%async_computation.5 | async-start | bytes 1572864 | tf_op jit(solution)/shard_map/all_to_all | solution.py:78
  53.4 1.6 copy-start.1
  55.0 8.8 %copy-start.3 = (f32[128]{0:T(128)S(1)}, f32[128]{0:T(128)}, u32[]{:S(2)}) copy-start(f32[128]{0:T(128)} %param.10) | copy-start | bytes 1540
  55.0 57.2 %all-to-all-start.2 = ((bf16[32,64,512]{2,1,0:T(8,128)(2,1)}), bf16[32,64,512]{2,1,0:T(8,128)(2,1)S(1)}, u32[]{:S(2)}, u32[]{:S(2)}) async-start(bf16[32,64,512]{2,1,0:T(8,128)(2,1)} %bitcast.73), calls=%async_computation.2 | async-start | bytes 4194304 | tf_op jit(solution)/shard_map/all_to_all | solution.py:61
  63.1 155.9 %all-gather.2.cloned.1.call-start = ((), (), s32[]{:S(2)}) async-start(), calls=%async_computation.8 | async-start | bytes 7077888 | tf_op jit(solution)/shard_map/all_gather | solution.py:79
  115.0 54.8 %all-to-all-start = ((bf16[32,128,256]{2,1,0:T(8,128)(2,1)}), bf16[32,128,256]{2,1,0:T(8,128)(2,1)}, u32[]{:S(2)}, u32[]{:S(2)}) async-start(bf16[32,128,256]{2,1,0:T(8,128)(2,1)} %bitcast.75), calls=%async_computation | async-start | bytes 4194304 | tf_op jit(solution)/shard_map/all_to_all | solution.py:51
  202.8 55.8 %all-to-all-start.1 = ((bf16[32,128,256]{2,1,0:T(8,128)(2,1)}), bf16[32,128,256]{2,1,0:T(8,128)(2,1)}, u32[]{:S(2)}, u32[]{:S(2)}) async-start(bf16[32,128,256]{2,1,0:T(8,128)(2,1)} %bitcast.74), calls=%async_computation.1 | async-start | bytes 4194304 | tf_op jit(solution)/shard_map/all_to_all | solution.py:58
  209.3 103.1 %reduce-scatter.2.cloned.1.call-start = ((), (), s32[]{:S(2)}) async-start(), calls=%async_computation.9 | async-start | bytes 7077888 | tf_op jit(solution)/shard_map/reduce_scatter | solution.py:87
  219.0 39.7 %copy-start = (bf16[1,256,8,512]{1,3,2,0:T(8,128)(2,1)S(1)}, bf16[1,256,8,512]{1,3,2,0:T(8,128)(2,1)}, u32[]{:S(2)}) copy-start(bf16[1,256,8,512]{1,3,2,0:T(8,128)(2,1)} %copy.55) | copy-start | bytes 6291460
  322.6 9.2 %copy-start.2 = (f32[192,2]{0,1:T(2,128)S(1)}, f32[192,2]{0,1:T(2,128)}, u32[]{:S(2)}) copy-start(f32[192,2]{0,1:T(2,128)} %param.9) | copy-start | bytes 4612
  324.1 27.4 %all-to-all-start.6 = ((bf16[16,2,12288]{2,1,0:T(2,128)(2,1)}), bf16[16,2,12288]{2,1,0:T(2,128)(2,1)S(1)}, u32[]{:S(2)}, u32[]{:S(2)}) async-start(bf16[16,2,12288]{2,1,0:T(2,128)(2,1)} %reshape.182), calls=%async_computation.7 | async-start | bytes 1572864 | tf_op jit(solution)/shard_map/all_to_all | solution.py:91
Sparse Core Ops, SparseCore 0:
  66.3 44.5 all-gather.1
  271.4 40.8 reduce-scatter.1
where the time goes:
time: 371 us; the launch traced here: 370 us
  waiting for transfers between devices  168 us (45%)
  local copies, waits for them, and re-layouts  63.2 us (17%)
  starting transfers between devices  41.8 us (11%)
  other arithmetic  33 us (9%)
  blocking collectives  31.4 us (8%)
  matrix products  18 us (5%)
  between operations  14.3 us (4%)
    all_to_all x1, waiting for transfers between devices, body(): lax.all_to_all(jnp.tile(down_cast, (copies, 1, 1)), ('gr', 'fs'), split_a...  44.7 us
    reduce_scatter x1, waiting for transfers between devices, body(): lax.psum_scatter(partial_value.astype(jnp.bfloat16), 'tp', scatter_dimens...  41.1 us
    all_to_all x1, waiting for transfers between devices, body(): lax.all_to_all(jnp.tile(up_cast, (copies, 1, 1)), ('gr', 'fs'), split_axi...  34.3 us
    all_to_all x1, blocking collectives, body(): lax.all_to_all(down_full, 'tp', split_axis=1, concat_axis=2, tiled=True)  31.4 us
    unnamed x19, local copies, waits for them, and re-layouts  23.7 us
    unnamed x2, other arithmetic  20.7 us
    all_to_all x1, waiting for transfers between devices, body(): lax.all_to_all(buffer, 'fs', split_axis=0, concat_axis=1, tiled=True)  19.2 us
    all_to_all x1, local copies, waits for them, and re-layouts, body(): lax.all_to_all(jnp.tile(down_cast, (copies, 1, 1)), ('gr', 'fs'), split_a...  18.5 us
  transfers between devices with their start and end apart: 8, of which 6 were waited for; matrix products, arithmetic and copies ran while one was open for 19% of the time, Pallas kernels for 0%

commit v1 on v0

v1 whole, which is shorter than its diff:
```python
import functools

import jax
import jax.numpy as jnp
from jax import lax
from jax.experimental import pallas as pl
from jax.experimental.pallas import tpu as pltpu
from jax.sharding import PartitionSpec as P

EPS = 1e-06
MESH = pl.DeviceIdType.MESH
F32 = jnp.float32
BF16 = jnp.bfloat16
NQ = 4


def kernel(
    dims,
    tok_ref, ids_ref, logit_ref, gain_ref, gate_hbm, up_hbm, down_hbm,
    gate_out, up_out, down_out, mixed_out,
    stage_g, stage_u, stage_d, snd_g, snd_u, snd_d,
    wg, wu, wd, slots, share_hi, share_lo, xall, hidden,
    psend, precv, ysum, yrecv, rsend, rrecv,
    load_sem, disp_s, disp_r, w_s, g_r, u_r, d_r,
    ag_s, ag_r, sib_s, sib_r, ps_s, ps_r, ys_s, ys_r, rt_s, rt_r, out_sem,
):
    n_gr, n_zl, n_x, n_y, n_c, cap = dims
    n_fs = n_zl * n_x
    n_z = n_gr * n_zl
    n_tp = n_y * n_c
    g = lax.axis_index("gr")
    f = lax.axis_index("fs")
    t = lax.axis_index("tp")
    z = g * n_zl + f // n_x
    x = f % n_x
    y = t // n_c
    c = t % n_c
    part = g * n_fs + f
    rows_g = stage_g.shape[1]
    rows_d = stage_d.shape[1]
    wide = tok_ref.shape[1]
    wq = wide // NQ
    n_rows = n_fs * cap
    n_peer = n_z * n_x
    d_model = n_tp * wide
    sibling = (g, f, y * n_c + (1 - c))

    def remote(src, dst, s_sem, r_sem, to):
        return pltpu.make_async_remote_copy(
            src_ref=src, dst_ref=dst, send_sem=s_sem, recv_sem=r_sem, device_id=to, device_id_type=MESH
        )

    def wait_recv(ref, sem):
        remote(ref, ref, sem, sem, sibling).wait_recv()

    def wait_send(ref, sem):
        remote(ref, ref, sem, sem, sibling).wait_send()

    def peer(i):
        a = i // n_x
        off = n_z // 2 + (1 - 2 * (a % 2)) * ((a + 1) // 2)
        zz = (z + off) % n_z
        xx = (x + 1 + i) % n_x
        return zz // n_zl, (zz % n_zl) * n_x + xx

    loads = [
        pltpu.make_async_copy(gate_hbm, stage_g, load_sem.at[0]),
        pltpu.make_async_copy(up_hbm, stage_u, load_sem.at[1]),
        pltpu.make_async_copy(down_hbm, stage_d, load_sem.at[2]),
    ]
    for copy in loads:
        copy.start()

    barrier = pltpu.get_barrier_semaphore()

    def greet(i, carry):
        pg, pf = peer(i)
        pl.semaphore_signal(barrier, inc=1, device_id=(pg, pf, t), device_id_type=MESH)
        return carry

    lax.fori_loop(0, n_peer - 1, greet, 0)

    def greet_down(i, carry):
        to = (t // n_zl, (t % n_zl) * n_x + i // n_tp, i % n_tp)
        mine = jnp.logical_and(z == t, jnp.logical_and(i // n_tp == x, i % n_tp == t))

        @pl.when(jnp.logical_not(mine))
        def _():
            pl.semaphore_signal(barrier, inc=1, device_id=to, device_id_type=MESH)

        return carry

    lax.fori_loop(0, n_x * n_tp, greet_down, 0)
    for dy in range(1, n_y):
        pl.semaphore_signal(barrier, inc=1, device_id=(g, f, ((y + dy) % n_y) * n_c + c), device_id_type=MESH)
    pl.semaphore_signal(barrier, inc=1, device_id=sibling, device_id_type=MESH)

    n_tok = tok_ref.shape[0]
    ids = ids_ref[...]
    sig = jax.nn.sigmoid(logit_ref[...])
    share = sig / jnp.sum(sig, axis=0, keepdims=True)
    experts = lax.broadcasted_iota(jnp.int32, (n_fs, n_tok), 0)
    hit0 = (ids[0:1, :] == experts).astype(F32)
    hit1 = (ids[1:2, :] == experts).astype(F32)
    member = hit0 + hit1
    weight = hit0 * share[0:1, :] + hit1 * share[1:2, :]
    earlier = (
        lax.broadcasted_iota(jnp.int32, (n_tok, n_tok), 0) < lax.broadcasted_iota(jnp.int32, (n_tok, n_tok), 1)
    ).astype(BF16)
    rank = jnp.dot(member.astype(BF16), earlier, preferred_element_type=F32)
    rank = jnp.where(member > 0.5, rank, -1.0)
    slot_no = lax.broadcasted_iota(jnp.int32, (cap, n_tok), 0).astype(F32)
    tok = tok_ref[...]
    for e in range(n_fs):
        pick = (slot_no == rank[e : e + 1, :]).astype(F32)
        slots[e * cap : (e + 1) * cap, :] = jnp.dot(
            pick.astype(BF16), tok, preferred_element_type=F32
        ).astype(BF16)
        scaled = pick * weight[e : e + 1, :]
        hi = scaled.astype(BF16)
        share_hi[e * cap : (e + 1) * cap, :] = hi
        share_lo[e * cap : (e + 1) * cap, :] = (scaled - hi.astype(F32)).astype(BF16)

    gcol = jnp.broadcast_to(gain_ref[...], (rows_g, rows_g)).T
    loads[0].wait()

    def cast_gate(e, carry):
        for h in range(0, stage_g.shape[2], rows_g):
            snd_g[e, :, h : h + rows_g] = (stage_g[e, :, h : h + rows_g] * gcol).astype(BF16)
        return carry

    lax.fori_loop(0, n_fs, cast_gate, 0)
    wg[pl.ds(pl.multiple_of(part * rows_g, rows_g), rows_g), :] = snd_g[f]
    loads[1].wait()

    def cast_up(e, carry):
        for h in range(0, stage_u.shape[2], rows_g):
            snd_u[e, :, h : h + rows_g] = (stage_u[e, :, h : h + rows_g] * gcol).astype(BF16)
        return carry

    lax.fori_loop(0, n_fs, cast_up, 0)
    wu[pl.ds(pl.multiple_of(part * rows_g, rows_g), rows_g), :] = snd_u[f]
    loads[2].wait()

    def cast_down(e, carry):
        for q in range(NQ):
            snd_d[q, e] = stage_d[e, :, q * wq : (q + 1) * wq].astype(BF16)
        return carry

    lax.fori_loop(0, n_fs, cast_down, 0)

    def down_place(q):
        return wd.at[
            pl.ds(pl.multiple_of(x * rows_d, rows_d), rows_d),
            pl.ds(pl.multiple_of(t * wide + q * wq, wq), wq),
        ]

    @pl.when(z == t)
    def _():
        for q in range(NQ):
            wd[
                pl.ds(pl.multiple_of(x * rows_d, rows_d), rows_d),
                pl.ds(pl.multiple_of(t * wide + q * wq, wq), wq),
            ] = snd_d[q, f]

    mine_x = xall.at[t, pl.ds(pl.multiple_of(f * cap, cap), cap), :]
    xall[t, pl.ds(pl.multiple_of(f * cap, cap), cap), :] = slots[pl.ds(pl.multiple_of(f * cap, cap), cap), :]

    pl.semaphore_wait(barrier, (n_peer - 1) + (n_y - 1) + 1 + n_peer - jnp.where(z == t, 1, 0))

    def dispatch(i, carry):
        to = (f + i) % n_fs
        remote(
            slots.at[pl.ds(pl.multiple_of(to * cap, cap), cap), :], mine_x, disp_s, disp_r, (g, to, t)
        ).start()
        return carry

    lax.fori_loop(1, n_fs, dispatch, 0)

    def send_gate(i, carry):
        pg, pf = peer(i)
        remote(
            snd_g.at[pf], wg.at[pl.ds(pl.multiple_of(part * rows_g, rows_g), rows_g), :], w_s.at[0], g_r, (pg, pf, t)
        ).start()
        return carry

    lax.fori_loop(0, n_peer - 1, send_gate, 0)

    wait_recv(xall.at[0, pl.ds(0, (n_fs - 1) * cap), :], disp_r)
    for dy in range(1, n_y):
        remote(xall.at[t], xall.at[t], ag_s, ag_r.at[n_y - dy], (g, f, ((y + dy) % n_y) * n_c + c)).start()
    remote(xall.at[t], xall.at[t], sib_s, sib_r.at[0], sibling).start()

    def send_up(i, carry):
        pg, pf = peer(i)
        remote(
            snd_u.at[pf], wu.at[pl.ds(pl.multiple_of(part * rows_g, rows_g), rows_g), :], w_s.at[1], u_r, (pg, pf, t)
        ).start()
        return carry

    lax.fori_loop(0, n_peer - 1, send_up, 0)
    for q in range(NQ):

        def send_down(i, carry, q=q):
            pg, pf = peer(i)
            remote(snd_d.at[q, pf], down_place(q), w_s.at[2], d_r.at[q], (pg, pf, z)).start()
            return carry

        lax.fori_loop(0, n_peer - 1, send_down, 0)

        @pl.when(z != t)
        def _(q=q):
            remote(snd_d.at[q, f], down_place(q), w_s.at[2], d_r.at[q], (g, f, z)).start()

    for dy in range(1, n_y):
        from_tp = ((y + dy) % n_y) * n_c + c
        wait_recv(xall.at[from_tp], ag_r.at[dy])
        remote(xall.at[from_tp], xall.at[from_tp], sib_s, sib_r.at[dy], sibling).start()
    for dy in range(n_y):
        from_tp = ((y + dy) % n_y) * n_c + (1 - c)
        wait_recv(xall.at[from_tp], sib_r.at[dy])
    wait_send(xall.at[pl.ds(0, n_y - 1)], ag_s)
    wait_send(xall.at[pl.ds(0, n_y)], sib_s)

    row_block = 32

    def normalize(i, carry):
        rows = pl.ds(pl.multiple_of(i * row_block, row_block), row_block)
        squares = jnp.zeros((row_block, wide), F32)
        for k in range(n_tp):
            v = xall[k, rows, :].astype(F32)
            squares = squares + v * v
        scale = lax.rsqrt(jnp.sum(squares, axis=1, keepdims=True) / d_model + EPS)
        for k in range(n_tp):
            xall[k, rows, :] = (xall[k, rows, :].astype(F32) * scale).astype(BF16)
        return carry

    lax.fori_loop(0, n_rows // row_block, normalize, 0)

    all_but_one = (n_peer - 1) * rows_g
    wait_recv(wg.at[pl.ds(0, all_but_one), :], g_r)
    gate_copy = pltpu.make_async_copy(wg, gate_out.at[0], out_sem.at[0])
    gate_copy.start()
    wait_recv(wu.at[pl.ds(0, all_but_one), :], u_r)
    up_copy = pltpu.make_async_copy(wu, up_out.at[0], out_sem.at[1])
    up_copy.start()
    scale_in = d_model ** (-0.5)
    mm_rows = 256

    def hidden_rows(i, carry):
        rows = pl.ds(pl.multiple_of(i * mm_rows, mm_rows), mm_rows)
        gate_sum = jnp.zeros((mm_rows, wg.shape[1]), F32)
        up_sum = jnp.zeros((mm_rows, wu.shape[1]), F32)
        for k in range(n_tp):
            v = xall[k, rows, :]
            gate_sum = gate_sum + jnp.dot(v, wg[k * wide : (k + 1) * wide, :], preferred_element_type=F32)
            up_sum = up_sum + jnp.dot(v, wu[k * wide : (k + 1) * wide, :], preferred_element_type=F32)
        gate_value = gate_sum * scale_in
        hidden[rows, :] = (gate_value * jax.nn.sigmoid(gate_value) * (up_sum * scale_in)).astype(BF16)
        return carry

    lax.fori_loop(0, n_rows // mm_rows, hidden_rows, 0)

    scale_out = (n_tp * wg.shape[1]) ** (-0.5)

    def partial(q, col_tp):
        cols = pl.ds(pl.multiple_of(col_tp * wide + q * wq, wq), wq)
        return jnp.dot(hidden[...], wd[:, cols], preferred_element_type=F32)

    def finish(q):
        for dy in range(1, n_y):
            wait_recv(yrecv.at[q, dy], ys_r.at[q, dy])
        total = ysum[q, y].astype(F32)
        for dy in range(1, n_y):
            total = total + yrecv[q, dy].astype(F32)
        rsend[q] = (total * scale_out).astype(BF16)

        rrecv[q, pl.ds(pl.multiple_of(f * cap, cap), cap), :] = rsend[q, pl.ds(pl.multiple_of(f * cap, cap), cap), :]

        def give(i, carry):
            to = (f + i) % n_fs
            remote(
                rsend.at[q, pl.ds(pl.multiple_of(to * cap, cap), cap), :],
                rrecv.at[q, pl.ds(pl.multiple_of(f * cap, cap), cap), :],
                rt_s, rt_r.at[q], (g, to, t),
            ).start()
            return carry

        lax.fori_loop(1, n_fs, give, 0)

    def combine(q):
        wait_recv(rrecv.at[q, pl.ds(0, (n_fs - 1) * cap), :], rt_r.at[q])
        dn = (((0,), (0,)), ((), ()))
        got = rrecv[q]
        out = lax.dot_general(share_hi[...], got, dn, preferred_element_type=F32)
        out = out + lax.dot_general(share_lo[...], got, dn, preferred_element_type=F32)
        mixed_out[:, q * wq : (q + 1) * wq] = out.astype(BF16)

    for q in range(NQ):

        @pl.when(z == t)
        def _(q=q):
            wait_recv(wg.at[pl.ds(0, all_but_one // NQ), :], d_r.at[q])

        @pl.when(z != t)
        def _(q=q):
            wait_recv(wg.at[pl.ds(0, wg.shape[0] // NQ), :], d_r.at[q])

        def for_sibling(yy, carry, q=q):
            psend[q, yy] = partial(q, yy * n_c + (1 - c)).astype(BF16)
            return carry

        lax.fori_loop(0, n_y, for_sibling, 0)
        remote(psend.at[q], precv.at[q], ps_s, ps_r.at[q], sibling).start()

        def for_own(yy, carry, q=q):
            ysum[q, yy] = partial(q, yy * n_c + c).astype(BF16)
            return carry

        lax.fori_loop(0, n_y, for_own, 0)
        if q > 0:
            finish(q - 1)
        wait_recv(precv.at[q], ps_r.at[q])

        def pair_sum(yy, carry, q=q):
            ysum[q, yy] = (ysum[q, yy].astype(F32) + precv[q, yy].astype(F32)).astype(BF16)
            return carry

        lax.fori_loop(0, n_y, pair_sum, 0)
        for dy in (2, 1, 3):
            yy = (y + dy) % n_y
            remote(ysum.at[q, yy], yrecv.at[q, n_y - dy], ys_s, ys_r.at[q, n_y - dy], (g, f, yy * n_c + c)).start()
        if q > 1:
            combine(q - 2)
    down_copy = pltpu.make_async_copy(wd, down_out.at[0], out_sem.at[2])
    down_copy.start()
    finish(NQ - 1)
    for q in range(max(NQ - 2, 0), NQ):
        combine(q)

    wait_send(slots.at[pl.ds(0, (n_fs - 1) * cap), :], disp_s)
    wait_send(wg.at[pl.ds(0, all_but_one), :], w_s.at[0])
    wait_send(wu.at[pl.ds(0, all_but_one), :], w_s.at[1])

    @pl.when(z == t)
    def _():
        wait_send(wg.at[pl.ds(0, all_but_one), :], w_s.at[2])

    @pl.when(z != t)
    def _():
        wait_send(wg, w_s.at[2])

    wait_send(psend, ps_s)
    wait_send(yrecv.at[:, pl.ds(0, n_y - 1)], ys_s)
    wait_send(rrecv.at[:, pl.ds(0, (n_fs - 1) * cap), :], rt_s)
    gate_copy.wait()
    up_copy.wait()
    down_copy.wait()


def body(tokens, route_ids, route_logits, gain, gate_master, up_master, down_master, *, sizes):
    n_gr, n_zl, n_x, n_y, n_c = sizes
    experts, rows_g, ff = gate_master.shape
    rows_d, wide = down_master.shape[1:]
    n_tok, top = route_ids.shape
    cap = 2 * n_tok * top // experts
    n_fs, n_tp = n_zl * n_x, n_y * n_c
    n_rows = n_fs * cap
    d_model, hid = wide * n_tp, ff
    wq = wide // NQ
    vmem = lambda *shape, dtype=BF16: pltpu.VMEM(shape, dtype)
    dma = pltpu.SemaphoreType.DMA
    any_spec = pl.BlockSpec(memory_space=pl.ANY)
    vmem_spec = pl.BlockSpec(memory_space=pltpu.VMEM)
    return pl.pallas_call(
        functools.partial(kernel, (n_gr, n_zl, n_x, n_y, n_c, cap)),
        out_shape=(
            jax.ShapeDtypeStruct((1, d_model, ff), BF16),
            jax.ShapeDtypeStruct((1, d_model, ff), BF16),
            jax.ShapeDtypeStruct((1, hid, d_model), BF16),
            jax.ShapeDtypeStruct((n_tok, wide), BF16),
        ),
        in_specs=[vmem_spec] * 4 + [any_spec] * 3,
        out_specs=(any_spec, any_spec, any_spec, vmem_spec),
        scratch_shapes=[
            vmem(experts, rows_g, ff, dtype=F32),
            vmem(experts, rows_g, ff, dtype=F32),
            vmem(experts, rows_d, wide, dtype=F32),
            vmem(experts, rows_g, ff),
            vmem(experts, rows_g, ff),
            vmem(NQ, experts, rows_d, wq),
            vmem(d_model, ff),
            vmem(d_model, ff),
            vmem(hid, d_model),
            vmem(n_rows, wide),
            vmem(n_rows, n_tok),
            vmem(n_rows, n_tok),
            vmem(n_tp, n_rows, wide),
            vmem(n_rows, hid),
            vmem(NQ, n_y, n_rows, wq),
            vmem(NQ, n_y, n_rows, wq),
            vmem(NQ, n_y, n_rows, wq),
            vmem(NQ, n_y, n_rows, wq),
            vmem(NQ, n_rows, wq),
            vmem(NQ, n_rows, wq),
            dma((3,)), dma, dma, dma((3,)), dma, dma, dma((NQ,)),
            dma, dma((n_y,)), dma, dma((n_y,)), dma, dma((NQ,)), dma, dma((NQ, n_y)), dma, dma((NQ,)), dma((3,)),
        ],
        compiler_params=pltpu.CompilerParams(
            collective_id=0, has_side_effects=True, vmem_limit_bytes=60 * 1024 * 1024
        ),
    )(tokens, route_ids.T, route_logits.T, gain[None, :], gate_master, up_master, down_master)


def solution(mesh):
    n_zl, n_x, n_c = 4, 4, 2
    sizes = (mesh.shape["gr"], n_zl, n_x, mesh.shape["tp"] // n_c, n_c)
    in_specs = (
        P(("gr", "fs"), "tp"),
        P(("gr", "fs"), None),
        P(("gr", "fs"), None),
        P(("gr", "fs")),
        P(None, ("gr", "fs"), "tp"),
        P(None, ("gr", "fs"), "tp"),
        P(None, ("gr", "fs"), "tp"),
    )
    out_specs = (
        P("fs", None, "tp"),
        P("fs", None, "tp"),
        P("fs", "tp", None),
        P(("gr", "fs"), "tp"),
    )
    return jax.shard_map(
        functools.partial(body, sizes=sizes), mesh=mesh, in_specs=in_specs, out_specs=out_specs, check_vma=False
    )
```

time: 371 us -> 222 us (0.60)
  Pallas kernels: 0 us -> 213 us
  waiting for transfers between devices: 168 us -> 0 us
  local copies, waits for them, and re-layouts: 63.2 us -> 7.54 us
  starting transfers between devices: 41.8 us -> 0 us
  other arithmetic: 33 us -> 0 us
  blocking collectives: 31.4 us -> 0 us
  matrix products: 18 us -> 0 us
  between operations: 14.3 us -> 0.65 us
    pallas_call x0 -> x1, Pallas kernels: none -> 213 us  [body(): pl.pallas_call(functools.partial(kernel, (n_gr, n_zl, n_x, n_y, n_c, cap)...]
    all_to_all x6 -> x0, waiting for transfers between devices: 126 us -> none  [the longest x1 44.7 us: body(): lax.all_to_all(jnp.tile(down_cast, (copies, 1, 1)), ('gr', 'fs'), split_a...]
    all_to_all x6 -> x0, starting transfers between devices: 41.7 us -> none  [the longest x1 8.48 us: body(): lax.all_to_all(buffer, 'fs', split_axis=0, concat_axis=1, tiled=True)]
    reduce_scatter x1 -> x0, waiting for transfers between devices: 41.1 us -> none  [body(): lax.psum_scatter(partial_value.astype(jnp.bfloat16), 'tp', scatter_dimens...]
    all_to_all x1 -> x0, blocking collectives: 31.4 us -> none  [body(): lax.all_to_all(down_full, 'tp', split_axis=1, concat_axis=2, tiled=True)]
    all_to_all x2 -> x0, local copies, waits for them, and re-layouts: 20.9 us -> none  [the longest x1 18.5 us: body(): lax.all_to_all(jnp.tile(down_cast, (copies, 1, 1)), ('gr', 'fs'), split_a...]
    unnamed x2 -> x0, other arithmetic: 20.7 us -> none
    dot_general x2 -> x0, matrix products: 18 us -> none  [the longest x1 12.7 us: body(): jnp.einsum('erf,efd->erd', hidden, down_rows, preferred_element_type=jnp....]
  transfers between devices with their start and end apart: 8 -> 0, of which waited for: 6 -> 0; matrix products, arithmetic and copies ran while one was open for 19% -> 0% of each run, Pallas kernels for 0% -> 0%
where the time goes in v1:
time: 222 us
  Pallas kernels  213 us (96%)
  local copies, waits for them, and re-layouts  7.54 us (3%)
    pallas_call x1, Pallas kernels, body(): pl.pallas_call(functools.partial(kernel, (n_gr, n_zl, n_x, n_y, n_c, cap)...  213 us
    unnamed x10, local copies, waits for them, and re-layouts  7.54 us

profile of v1, /device:TPU:32, one launch (start us, length us, event | category | flops | bytes accessed | tf_op | source)
XLA Modules:
  0.0 221.5 jit_solution(939882590689989895)
XLA Ops:
  0.6 213.3 %shard_map.102 = (bf16[1,4096,256]{2,1,0:T(8,128)(2,1)}, bf16[1,4096,256]{2,1,0:T(8,128)(2,1)}, bf16[1,256,4096]{2,1,0:T(8,128)(2,1)}, bf16[192,512]{1,0:T(8,128)(2,1)}) custom-call(bf16[192,512]{1,0:T(8,128)(2,1)} %tok_ref.1, s32[2,192]{1,0:T(2,128)} %bitcast.3, f32[2,192]{1,0:T(2,128)} %bitcast.4, f32[1,128]{1,0:T(1,128)} %bitcast.5, ...), custom_call_target="tpu_custom_call" | custom-call | tf_op jit(solution)/shard_map/pallas_call | solution.py:375
  214.0 0.0 copy-start.1
  214.0 3.2 %copy.15 = bf16[1,4096,256]{2,1,0:T(8,128)(2,1)} copy(bf16[1,4096,256]{2,1,0:T(8,128)(2,1)} %get-tuple-element.8) | data formatting | bytes 4194304
  217.2 0.0 copy-done.1
  217.2 0.0 copy-start
  217.2 1.3 copy.16
  218.5 1.0 copy-done
  219.5 0.0 copy-start.2
  219.5 1.3 copy.17
  220.8 0.0 copy-done.2
  220.8 0.7 copy.18
Async XLA Ops:
  214.0 3.2 %copy-start.1 = (bf16[1,4096,256]{2,1,0:T(8,128)(2,1)S(1)}, bf16[1,4096,256]{2,1,0:T(8,128)(2,1)}, u32[]{:S(2)}) copy-start(bf16[1,4096,256]{2,1,0:T(8,128)(2,1)} %get-tuple-element.9) | copy-start | bytes 6291460
  217.2 2.3 %copy-start = (bf16[1,256,4096]{2,1,0:T(8,128)(2,1)S(1)}, bf16[1,256,4096]{2,1,0:T(8,128)(2,1)}, u32[]{:S(2)}) copy-start(bf16[1,256,4096]{2,1,0:T(8,128)(2,1)} %get-tuple-element.10) | copy-start | bytes 6291460
  219.5 1.3 copy-start.2

commit v2 on v1

--- a/solution.py
+++ b/solution.py
@@ -12,19 +12,21 @@
 F32 = jnp.float32
 BF16 = jnp.bfloat16
 NQ = 4
+NR = 4
 
 
 def kernel(
     dims,
     tok_ref, ids_ref, logit_ref, gain_ref, gate_hbm, up_hbm, down_hbm,
-    gate_out, up_out, down_out, mixed_out,
+    wg_out, wu_out, wd_out, mixed_out,
     stage_g, stage_u, stage_d, snd_g, snd_u, snd_d,
-    wg, wu, wd, slots, share_hi, share_lo, xall, hidden,
+    slots, share_hi, share_lo, xall, hidden,
     psend, precv, ysum, yrecv, rsend, rrecv,
     load_sem, disp_s, disp_r, w_s, g_r, u_r, d_r,
-    ag_s, ag_r, sib_s, sib_r, ps_s, ps_r, ys_s, ys_r, rt_s, rt_r, out_sem,
+    ag_s, ag_r, sib_s, sib_r, ps_s, ps_r, ys_s, ys_r, rt_s, rt_r,
 ):
     n_gr, n_zl, n_x, n_y, n_c, cap = dims
+    wg, wu, wd = wg_out.at[0], wu_out.at[0], wd_out.at[0]
     n_fs = n_zl * n_x
     n_z = n_gr * n_zl
     n_tp = n_y * n_c
@@ -56,11 +58,11 @@
     def wait_send(ref, sem):
         remote(ref, ref, sem, sem, sibling).wait_send()
 
-    def peer(i):
-        a = i // n_x
+    def peer(i, turn=0):
+        a = i % n_z
         off = n_z // 2 + (1 - 2 * (a % 2)) * ((a + 1) // 2)
         zz = (z + off) % n_z
-        xx = (x + 1 + i) % n_x
+        xx = (x + 1 + i // n_z + turn) % n_x
         return zz // n_zl, (zz % n_zl) * n_x + xx
 
     loads = [
@@ -199,19 +201,6 @@
         return carry
 
     lax.fori_loop(0, n_peer - 1, send_up, 0)
-    for q in range(NQ):
-
-        def send_down(i, carry, q=q):
-            pg, pf = peer(i)
-            remote(snd_d.at[q, pf], down_place(q), w_s.at[2], d_r.at[q], (pg, pf, z)).start()
-            return carry
-
-        lax.fori_loop(0, n_peer - 1, send_down, 0)
-
-        @pl.when(z != t)
-        def _(q=q):
-            remote(snd_d.at[q, f], down_place(q), w_s.at[2], d_r.at[q], (g, f, z)).start()
-
     for dy in range(1, n_y):
         from_tp = ((y + dy) % n_y) * n_c + c
         wait_recv(xall.at[from_tp], ag_r.at[dy])
@@ -237,13 +226,25 @@
 
     lax.fori_loop(0, n_rows // row_block, normalize, 0)
 
+    def start_down(q):
+        def send_down(i, carry):
+            pg, pf = peer(i, y)
+            here = jnp.logical_and(jnp.logical_and(pg == g, pf == f), t == z)
+
+            @pl.when(jnp.logical_not(here))
+            def _():
+                remote(snd_d.at[q, pf], down_place(q), w_s.at[2], d_r.at[q], (pg, pf, z)).start()
+
+            return carry
+
+        lax.fori_loop(0, n_peer, send_down, 0)
+
+    for q in range(2):
+        start_down(q)
+
     all_but_one = (n_peer - 1) * rows_g
     wait_recv(wg.at[pl.ds(0, all_but_one), :], g_r)
-    gate_copy = pltpu.make_async_copy(wg, gate_out.at[0], out_sem.at[0])
-    gate_copy.start()
     wait_recv(wu.at[pl.ds(0, all_but_one), :], u_r)
-    up_copy = pltpu.make_async_copy(wu, up_out.at[0], out_sem.at[1])
-    up_copy.start()
     scale_in = d_model ** (-0.5)
     mm_rows = 256
 
@@ -263,30 +264,41 @@
 
     scale_out = (n_tp * wg.shape[1]) ** (-0.5)
 
-    def partial(q, col_tp):
+    piece = n_rows // NR
+    per_piece = n_fs // NR
+
+    def partial(q, r, col_tp):
+        rows = pl.ds(pl.multiple_of(r * piece, piece), piece)
         cols = pl.ds(pl.multiple_of(col_tp * wide + q * wq, wq), wq)
-        return jnp.dot(hidden[...], wd[:, cols], preferred_element_type=F32)
+        return jnp.dot(hidden[rows, :], wd[:, cols], preferred_element_type=F32)
 
     def finish(q):
-        for dy in range(1, n_y):
-            wait_recv(yrecv.at[q, dy], ys_r.at[q, dy])
-        total = ysum[q, y].astype(F32)
-        for dy in range(1, n_y):
-            total = total + yrecv[q, dy].astype(F32)
-        rsend[q] = (total * scale_out).astype(BF16)
-
-        rrecv[q, pl.ds(pl.multiple_of(f * cap, cap), cap), :] = rsend[q, pl.ds(pl.multiple_of(f * cap, cap), cap), :]
-
-        def give(i, carry):
-            to = (f + i) % n_fs
-            remote(
-                rsend.at[q, pl.ds(pl.multiple_of(to * cap, cap), cap), :],
-                rrecv.at[q, pl.ds(pl.multiple_of(f * cap, cap), cap), :],
-                rt_s, rt_r.at[q], (g, to, t),
-            ).start()
+        def one(r, carry):
+            wait_recv(yrecv.at[q, r, pl.ds(0, n_y - 1)], ys_r.at[q, r])
+            total = ysum[q, r, y].astype(F32)
+            for dy in range(1, n_y):
+                total = total + yrecv[q, r, dy].astype(F32)
+            rsend[q, pl.ds(pl.multiple_of(r * piece, piece), piece), :] = (total * scale_out).astype(BF16)
+
+            def give(i, carry):
+                to = r * per_piece + i
+                block = pl.ds(pl.multiple_of(to * cap, cap), cap)
+                mine = pl.ds(pl.multiple_of(f * cap, cap), cap)
+
+                @pl.when(to == f)
+                def _():
+                    rrecv[q, mine, :] = rsend[q, mine, :]
+
+                @pl.when(to != f)
+                def _():
+                    remote(rsend.at[q, block, :], rrecv.at[q, mine, :], rt_s, rt_r.at[q], (g, to, t)).start()
+
+                return carry
+
+            lax.fori_loop(0, per_piece, give, 0)
             return carry
 
-        lax.fori_loop(1, n_fs, give, 0)
+        lax.fori_loop(0, NR, one, 0)
 
     def combine(q):
         wait_recv(rrecv.at[q, pl.ds(0, (n_fs - 1) * cap), :], rt_r.at[q])
@@ -306,34 +318,39 @@
         def _(q=q):
             wait_recv(wg.at[pl.ds(0, wg.shape[0] // NQ), :], d_r.at[q])
 
-        def for_sibling(yy, carry, q=q):
-            psend[q, yy] = partial(q, yy * n_c + (1 - c)).astype(BF16)
+        def for_sibling(r, carry, q=q):
+            for yy in range(n_y):
+                psend[q, r, yy] = partial(q, r, yy * n_c + (1 - c)).astype(BF16)
+            remote(psend.at[q, r], precv.at[q, r], ps_s, ps_r.at[q, r], sibling).start()
             return carry
 
-        lax.fori_loop(0, n_y, for_sibling, 0)
-        remote(psend.at[q], precv.at[q], ps_s, ps_r.at[q], sibling).start()
-
-        def for_own(yy, carry, q=q):
-            ysum[q, yy] = partial(q, yy * n_c + c).astype(BF16)
+        if q + 2 < NQ:
+            start_down(q + 2)
+        lax.fori_loop(0, NR, for_sibling, 0)
+
+        def for_own(r, carry, q=q):
+            for yy in range(n_y):
+                ysum[q, r, yy] = partial(q, r, yy * n_c + c).astype(BF16)
             return carry
 
-        lax.fori_loop(0, n_y, for_own, 0)
+        lax.fori_loop(0, NR, for_own, 0)
         if q > 0:
             finish(q - 1)
-        wait_recv(precv.at[q], ps_r.at[q])
-
-        def pair_sum(yy, carry, q=q):
-            ysum[q, yy] = (ysum[q, yy].astype(F32) + precv[q, yy].astype(F32)).astype(BF16)
+
+        def exchange(r, carry, q=q):
+            wait_recv(precv.at[q, r], ps_r.at[q, r])
+            for yy in range(n_y):
+                ysum[q, r, yy] = (ysum[q, r, yy].astype(F32) + precv[q, r, yy].astype(F32)).astype(BF16)
+            for dy in (2, 1, 3):
+                yy = (y + dy) % n_y
+                remote(
+                    ysum.at[q, r, yy], yrecv.at[q, r, n_y - dy], ys_s, ys_r.at[q, r], (g, f, yy * n_c + c)
+                ).start()
             return carry
 
-        lax.fori_loop(0, n_y, pair_sum, 0)
-        for dy in (2, 1, 3):
-            yy = (y + dy) % n_y
-            remote(ysum.at[q, yy], yrecv.at[q, n_y - dy], ys_s, ys_r.at[q, n_y - dy], (g, f, yy * n_c + c)).start()
+        lax.fori_loop(0, NR, exchange, 0)
         if q > 1:
             combine(q - 2)
-    down_copy = pltpu.make_async_copy(wd, down_out.at[0], out_sem.at[2])
-    down_copy.start()
     finish(NQ - 1)
     for q in range(max(NQ - 2, 0), NQ):
         combine(q)
@@ -351,11 +368,18 @@
         wait_send(wg, w_s.at[2])
 
     wait_send(psend, ps_s)
-    wait_send(yrecv.at[:, pl.ds(0, n_y - 1)], ys_s)
+    wait_send(yrecv.at[:, :, pl.ds(0, n_y - 1)], ys_s)
     wait_send(rrecv.at[:, pl.ds(0, (n_fs - 1) * cap), :], rt_s)
-    gate_copy.wait()
-    up_copy.wait()
-    down_copy.wait()
+
+
+def write_out(*refs):
+    n = len(refs) // 2
+    srcs, dsts, sem = refs[:n], refs[n : 2 * n], refs[2 * n]
+    copies = [pltpu.make_async_copy(src, dst, sem.at[i]) for i, (src, dst) in enumerate(zip(srcs, dsts))]
+    for copy in copies:
+        copy.start()
+    for copy in copies:
+        copy.wait()
 
 
 def body(tokens, route_ids, route_logits, gain, gate_master, up_master, down_master, *, sizes):
@@ -372,16 +396,16 @@
     dma = pltpu.SemaphoreType.DMA
     any_spec = pl.BlockSpec(memory_space=pl.ANY)
     vmem_spec = pl.BlockSpec(memory_space=pltpu.VMEM)
-    return pl.pallas_call(
+    results = pl.pallas_call(
         functools.partial(kernel, (n_gr, n_zl, n_x, n_y, n_c, cap)),
         out_shape=(
-            jax.ShapeDtypeStruct((1, d_model, ff), BF16),
-            jax.ShapeDtypeStruct((1, d_model, ff), BF16),
-            jax.ShapeDtypeStruct((1, hid, d_model), BF16),
-            jax.ShapeDtypeStruct((n_tok, wide), BF16),
+            pltpu.VMEM((1, d_model, ff), BF16),
+            pltpu.VMEM((1, d_model, ff), BF16),
+            pltpu.VMEM((1, hid, d_model), BF16),
+            pltpu.VMEM((n_tok, wide), BF16),
         ),
         in_specs=[vmem_spec] * 4 + [any_spec] * 3,
-        out_specs=(any_spec, any_spec, any_spec, vmem_spec),
+        out_specs=(vmem_spec,) * 4,
         scratch_shapes=[
             vmem(experts, rows_g, ff, dtype=F32),
             vmem(experts, rows_g, ff, dtype=F32),
@@ -389,27 +413,32 @@
             vmem(experts, rows_g, ff),
             vmem(experts, rows_g, ff),
             vmem(NQ, experts, rows_d, wq),
-            vmem(d_model, ff),
-            vmem(d_model, ff),
-            vmem(hid, d_model),
             vmem(n_rows, wide),
             vmem(n_rows, n_tok),
             vmem(n_rows, n_tok),
             vmem(n_tp, n_rows, wide),
             vmem(n_rows, hid),
-            vmem(NQ, n_y, n_rows, wq),
-            vmem(NQ, n_y, n_rows, wq),
-            vmem(NQ, n_y, n_rows, wq),
-            vmem(NQ, n_y, n_rows, wq),
+            vmem(NQ, NR, n_y, n_rows // NR, wq),
+            vmem(NQ, NR, n_y, n_rows // NR, wq),
+            vmem(NQ, NR, n_y, n_rows // NR, wq),
+            vmem(NQ, NR, n_y, n_rows // NR, wq),
             vmem(NQ, n_rows, wq),
             vmem(NQ, n_rows, wq),
             dma((3,)), dma, dma, dma((3,)), dma, dma, dma((NQ,)),
-            dma, dma((n_y,)), dma, dma((n_y,)), dma, dma((NQ,)), dma, dma((NQ, n_y)), dma, dma((NQ,)), dma((3,)),
+            dma, dma((n_y,)), dma, dma((n_y,)), dma, dma((NQ, NR)), dma, dma((NQ, NR)), dma, dma((NQ,)),
         ],
         compiler_params=pltpu.CompilerParams(
-            collective_id=0, has_side_effects=True, vmem_limit_bytes=60 * 1024 * 1024
+            collective_id=0, has_side_effects=True, vmem_limit_bytes=50 * 1024 * 1024
         ),
     )(tokens, route_ids.T, route_logits.T, gain[None, :], gate_master, up_master, down_master)
+    return pl.pallas_call(
+        write_out,
+        out_shape=tuple(jax.ShapeDtypeStruct(r.shape, r.dtype) for r in results),
+        in_specs=[vmem_spec] * 4,
+        out_specs=(any_spec,) * 4,
+        scratch_shapes=[dma((4,))],
+        compiler_params=pltpu.CompilerParams(vmem_limit_bytes=1024 * 1024),
+    )(*(pltpu.with_memory_space_constraint(r, pltpu.VMEM) for r in results))
 
 
 def solution(mesh):

time: 222 us -> 203 us (0.914)
  Pallas kernels: 213 us -> 201 us
  local copies, waits for them, and re-layouts: 7.54 us -> 0 us
    pallas_call x1, Pallas kernels: 213 us -> 199 us  [body(): pl.pallas_call(functools.partial(kernel, (n_gr, n_zl, n_x, n_y, n_c, cap)...]
    unnamed x10 -> x0, local copies, waits for them, and re-layouts: 7.54 us -> none
    pallas_call x0 -> x1, Pallas kernels: none -> 2.74 us  [body(): pl.pallas_call(write_out, out_shape=tuple((jax.ShapeDtypeStruct(r.shape,...]
where the time goes in v2:
time: 203 us; the launch traced here: 202 us
  Pallas kernels  201 us (99%)
    pallas_call x1, Pallas kernels, body(): pl.pallas_call(functools.partial(kernel, (n_gr, n_zl, n_x, n_y, n_c, cap)...  199 us

profile of v2, /device:TPU:32, one launch (start us, length us, event | category | flops | bytes accessed | tf_op | source)
XLA Modules:
  0.0 202.1 jit_solution(2256733875266195274)
XLA Ops:
  0.6 198.7 %shard_map.102 = (bf16[1,4096,256]{2,1,0:T(8,128)(2,1)S(1)}, bf16[1,4096,256]{2,1,0:T(8,128)(2,1)S(1)}, bf16[1,256,4096]{2,1,0:T(8,128)(2,1)S(1)}, bf16[192,512]{1,0:T(8,128)(2,1)S(1)}) custom-call(bf16[192,512]{1,0:T(8,128)(2,1)} %tok_ref.1, s32[2,192]{1,0:T(2,128)} %bitcast.3, f32[2,192]{1,0:T(2,128)} %bitcast.4, f32[1,128]{1,0:T(1,128)} %bitcast.5, ...), custom_call_target="tpu_custom_call" | custom-call | tf_op jit(solution)/shard_map/pallas_call | solution.py:399
  199.3 2.7 %shard_map.103 = (bf16[1,4096,256]{2,1,0:T(8,128)(2,1)}, bf16[1,4096,256]{2,1,0:T(8,128)(2,1)}, bf16[1,256,4096]{2,1,0:T(8,128)(2,1)}, bf16[192,512]{1,0:T(8,128)(2,1)}) custom-call(bf16[1,4096,256]{2,1,0:T(8,128)(2,1)S(1)} %get-tuple-element.8.refs_0_, bf16[1,4096,256]{2,1,0:T(8,128)(2,1)S(1)} %get-tuple-element.9.refs_1_, ...), custom_call_target="tpu_custom_call" | custom-call | tf_op jit(solution)/shard_map/pallas_call | solution.py:434

commit v3 on v2

--- a/solution.py
+++ b/solution.py
@@ -17,13 +17,14 @@
 
 def kernel(
     dims,
-    tok_ref, ids_ref, logit_ref, gain_ref, gate_hbm, up_hbm, down_hbm,
+    tok_hbm, ids_hbm, logit_hbm, gain_hbm, gate_hbm, up_hbm, down_hbm,
     wg_out, wu_out, wd_out, mixed_out,
     stage_g, stage_u, stage_d, snd_g, snd_u, snd_d,
-    slots, share_hi, share_lo, xall, hidden,
-    psend, precv, ysum, yrecv, rsend, rrecv,
+    slots, share_hi, share_lo, xall, gate_act, hidden,
+    tok_ref, ids_ref, logit_ref, gain_ref,
+    psend, precv, ysum, passing, yrecv, rsend, rrecv,
     load_sem, disp_s, disp_r, w_s, g_r, u_r, d_r,
-    ag_s, ag_r, sib_s, sib_r, ps_s, ps_r, ys_s, ys_r, rt_s, rt_r,
+    ag_s, ag_r, sib_s, sib_r, ps_s, ps_r, ys_s, ps_y, ys_r, rt_s, rt_r,
 ):
     n_gr, n_zl, n_x, n_y, n_c, cap = dims
     wg, wu, wd = wg_out.at[0], wu_out.at[0], wd_out.at[0]
@@ -70,7 +71,13 @@
         pltpu.make_async_copy(up_hbm, stage_u, load_sem.at[1]),
         pltpu.make_async_copy(down_hbm, stage_d, load_sem.at[2]),
     ]
-    for copy in loads:
+    small = [
+        pltpu.make_async_copy(src, dst, load_sem.at[3 + i])
+        for i, (src, dst) in enumerate(
+            ((tok_hbm, tok_ref), (ids_hbm, ids_ref), (logit_hbm, logit_ref), (gain_hbm, gain_ref))
+        )
+    ]
+    for copy in small + loads:
         copy.start()
 
     barrier = pltpu.get_barrier_semaphore()
@@ -97,6 +104,8 @@
         pl.semaphore_signal(barrier, inc=1, device_id=(g, f, ((y + dy) % n_y) * n_c + c), device_id_type=MESH)
     pl.semaphore_signal(barrier, inc=1, device_id=sibling, device_id_type=MESH)
 
+    for copy in small:
+        copy.wait()
     n_tok = tok_ref.shape[0]
     ids = ids_ref[...]
     sig = jax.nn.sigmoid(logit_ref[...])
@@ -171,13 +180,15 @@
     pl.semaphore_wait(barrier, (n_peer - 1) + (n_y - 1) + 1 + n_peer - jnp.where(z == t, 1, 0))
 
     def dispatch(i, carry):
-        to = (f + i) % n_fs
+        a = i % n_zl
+        off = n_zl // 2 + (2 * (a % 2) - 1) * ((a + 1) // 2)
+        to = (f // n_x + off) % n_zl * n_x + (x + 1 + i // n_zl) % n_x
         remote(
             slots.at[pl.ds(pl.multiple_of(to * cap, cap), cap), :], mine_x, disp_s, disp_r, (g, to, t)
         ).start()
         return carry
 
-    lax.fori_loop(1, n_fs, dispatch, 0)
+    lax.fori_loop(0, n_fs - 1, dispatch, 0)
 
     def send_gate(i, carry):
         pg, pf = peer(i)
@@ -244,20 +255,27 @@
 
     all_but_one = (n_peer - 1) * rows_g
     wait_recv(wg.at[pl.ds(0, all_but_one), :], g_r)
-    wait_recv(wu.at[pl.ds(0, all_but_one), :], u_r)
     scale_in = d_model ** (-0.5)
     mm_rows = 256
 
+    def product(w, rows):
+        total = jnp.zeros((mm_rows, w.shape[1]), F32)
+        for k in range(n_tp):
+            total = total + jnp.dot(xall[k, rows, :], w[k * wide : (k + 1) * wide, :], preferred_element_type=F32)
+        return total * scale_in
+
+    def gate_rows(i, carry):
+        rows = pl.ds(pl.multiple_of(i * mm_rows, mm_rows), mm_rows)
+        gate_value = product(wg, rows)
+        gate_act[rows, :] = gate_value * jax.nn.sigmoid(gate_value)
+        return carry
+
+    lax.fori_loop(0, n_rows // mm_rows, gate_rows, 0)
+    wait_recv(wu.at[pl.ds(0, all_but_one), :], u_r)
+
     def hidden_rows(i, carry):
         rows = pl.ds(pl.multiple_of(i * mm_rows, mm_rows), mm_rows)
-        gate_sum = jnp.zeros((mm_rows, wg.shape[1]), F32)
-        up_sum = jnp.zeros((mm_rows, wu.shape[1]), F32)
-        for k in range(n_tp):
-            v = xall[k, rows, :]
-            gate_sum = gate_sum + jnp.dot(v, wg[k * wide : (k + 1) * wide, :], preferred_element_type=F32)
-            up_sum = up_sum + jnp.dot(v, wu[k * wide : (k + 1) * wide, :], preferred_element_type=F32)
-        gate_value = gate_sum * scale_in
-        hidden[rows, :] = (gate_value * jax.nn.sigmoid(gate_value) * (up_sum * scale_in)).astype(BF16)
+        hidden[rows, :] = (gate_act[rows, :] * product(wu, rows)).astype(BF16)
         return carry
 
     lax.fori_loop(0, n_rows // mm_rows, hidden_rows, 0)
@@ -266,6 +284,10 @@
 
     piece = n_rows // NR
     per_piece = n_fs // NR
+
+    def ring(r):
+        step = 1 - 2 * (r % 2)
+        return (y + n_y + step) % n_y, (y + n_y - step) % n_y, (y + n_y // 2) % n_y
 
     def partial(q, r, col_tp):
         rows = pl.ds(pl.multiple_of(r * piece, piece), piece)
@@ -274,10 +296,8 @@
 
     def finish(q):
         def one(r, carry):
-            wait_recv(yrecv.at[q, r, pl.ds(0, n_y - 1)], ys_r.at[q, r])
-            total = ysum[q, r, y].astype(F32)
-            for dy in range(1, n_y):
-                total = total + yrecv[q, r, dy].astype(F32)
+            wait_recv(yrecv.at[q, r], ys_r.at[q, r])
+            total = ysum[q, r, y].astype(F32) + yrecv[q, r, 0].astype(F32) + yrecv[q, r, 1].astype(F32)
             rsend[q, pl.ds(pl.multiple_of(r * piece, piece), piece), :] = (total * scale_out).astype(BF16)
 
             def give(i, carry):
@@ -299,6 +319,16 @@
             return carry
 
         lax.fori_loop(0, NR, one, 0)
+
+    def pass_chunk(q):
+        def pass_on(r, carry):
+            wait_recv(passing.at[q, r], ps_y.at[q, r])
+            ahead, _, _ = ring(r)
+            ysum[q, r, ahead] = (ysum[q, r, ahead].astype(F32) + passing[q, r].astype(F32)).astype(BF16)
+            remote(ysum.at[q, r, ahead], yrecv.at[q, r, 1], ys_s, ys_r.at[q, r], (g, f, ahead * n_c + c)).start()
+            return carry
+
+        lax.fori_loop(0, NR, pass_on, 0)
 
     def combine(q):
         wait_recv(rrecv.at[q, pl.ds(0, (n_fs - 1) * cap), :], rt_r.at[q])
@@ -334,25 +364,27 @@
             return carry
 
         lax.fori_loop(0, NR, for_own, 0)
-        if q > 0:
-            finish(q - 1)
 
         def exchange(r, carry, q=q):
             wait_recv(precv.at[q, r], ps_r.at[q, r])
             for yy in range(n_y):
                 ysum[q, r, yy] = (ysum[q, r, yy].astype(F32) + precv[q, r, yy].astype(F32)).astype(BF16)
-            for dy in (2, 1, 3):
-                yy = (y + dy) % n_y
-                remote(
-                    ysum.at[q, r, yy], yrecv.at[q, r, n_y - dy], ys_s, ys_r.at[q, r], (g, f, yy * n_c + c)
-                ).start()
+            ahead, behind, far = ring(r)
+            remote(ysum.at[q, r, far], passing.at[q, r], ys_s, ps_y.at[q, r], (g, f, ahead * n_c + c)).start()
+            remote(ysum.at[q, r, behind], yrecv.at[q, r, 0], ys_s, ys_r.at[q, r], (g, f, behind * n_c + c)).start()
             return carry
 
         lax.fori_loop(0, NR, exchange, 0)
+        if q > 0:
+            pass_chunk(q - 1)
         if q > 1:
-            combine(q - 2)
-    finish(NQ - 1)
+            finish(q - 2)
+        if q > 2:
+            combine(q - 3)
+    pass_chunk(NQ - 1)
     for q in range(max(NQ - 2, 0), NQ):
+        finish(q)
+    for q in range(max(NQ - 3, 0), NQ):
         combine(q)
 
     wait_send(slots.at[pl.ds(0, (n_fs - 1) * cap), :], disp_s)
@@ -368,7 +400,7 @@
         wait_send(wg, w_s.at[2])
 
     wait_send(psend, ps_s)
-    wait_send(yrecv.at[:, :, pl.ds(0, n_y - 1)], ys_s)
+    wait_send(ysum.at[:, :, pl.ds(0, n_y - 1)], ys_s)
     wait_send(rrecv.at[:, pl.ds(0, (n_fs - 1) * cap), :], rt_s)
 
 
@@ -404,7 +436,7 @@
             pltpu.VMEM((1, hid, d_model), BF16),
             pltpu.VMEM((n_tok, wide), BF16),
         ),
-        in_specs=[vmem_spec] * 4 + [any_spec] * 3,
+        in_specs=[any_spec] * 7,
         out_specs=(vmem_spec,) * 4,
         scratch_shapes=[
             vmem(experts, rows_g, ff, dtype=F32),
@@ -417,15 +449,21 @@
             vmem(n_rows, n_tok),
             vmem(n_rows, n_tok),
             vmem(n_tp, n_rows, wide),
+            vmem(n_rows, hid, dtype=F32),
             vmem(n_rows, hid),
+            vmem(n_tok, wide),
+            vmem(top, n_tok, dtype=jnp.int32),
+            vmem(top, n_tok, dtype=F32),
+            vmem(1, rows_g, dtype=F32),
             vmem(NQ, NR, n_y, n_rows // NR, wq),
             vmem(NQ, NR, n_y, n_rows // NR, wq),
             vmem(NQ, NR, n_y, n_rows // NR, wq),
-            vmem(NQ, NR, n_y, n_rows // NR, wq),
+            vmem(NQ, NR, n_rows // NR, wq),
+            vmem(NQ, NR, 2, n_rows // NR, wq),
             vmem(NQ, n_rows, wq),
             vmem(NQ, n_rows, wq),
-            dma((3,)), dma, dma, dma((3,)), dma, dma, dma((NQ,)),
-            dma, dma((n_y,)), dma, dma((n_y,)), dma, dma((NQ, NR)), dma, dma((NQ, NR)), dma, dma((NQ,)),
+            dma((7,)), dma, dma, dma((3,)), dma, dma, dma((NQ,)),
+            dma, dma((n_y,)), dma, dma((n_y,)), dma, dma((NQ, NR)), dma, dma((NQ, NR)), dma((NQ, NR)), dma, dma((NQ,)),
         ],
         compiler_params=pltpu.CompilerParams(
             collective_id=0, has_side_effects=True, vmem_limit_bytes=50 * 1024 * 1024

time: 203 us -> 196 us (0.966)
  Pallas kernels: 201 us -> 195 us
    pallas_call x1, Pallas kernels: 199 us -> 193 us  [body(): pl.pallas_call(functools.partial(kernel, (n_gr, n_zl, n_x, n_y, n_c, cap)...]
where the time goes in v3:
time: 196 us
  Pallas kernels  195 us (99%)
    pallas_call x1, Pallas kernels, body(): pl.pallas_call(functools.partial(kernel, (n_gr, n_zl, n_x, n_y, n_c, cap)...  193 us

profile of v3, /device:TPU:32, one launch (start us, length us, event | category | flops | bytes accessed | tf_op | source)
XLA Modules:
  0.0 196.0 jit_solution(7032498363287328617)
XLA Ops:
  0.6 192.6 %shard_map.102 = (bf16[1,4096,256]{2,1,0:T(8,128)(2,1)S(1)}, bf16[1,4096,256]{2,1,0:T(8,128)(2,1)S(1)}, bf16[1,256,4096]{2,1,0:T(8,128)(2,1)S(1)}, bf16[192,512]{1,0:T(8,128)(2,1)S(1)}) custom-call(bf16[192,512]{1,0:T(8,128)(2,1)} %tok_hbm.1, s32[2,192]{1,0:T(2,128)} %bitcast.3, f32[2,192]{1,0:T(2,128)} %bitcast.4, f32[1,128]{1,0:T(1,128)} %bitcast.5, ...), custom_call_target="tpu_custom_call" | custom-call | tf_op jit(solution)/shard_map/pallas_call | solution.py:431
  193.3 2.7 %shard_map.103 = (bf16[1,4096,256]{2,1,0:T(8,128)(2,1)}, bf16[1,4096,256]{2,1,0:T(8,128)(2,1)}, bf16[1,256,4096]{2,1,0:T(8,128)(2,1)}, bf16[192,512]{1,0:T(8,128)(2,1)}) custom-call(bf16[1,4096,256]{2,1,0:T(8,128)(2,1)S(1)} %get-tuple-element.8.refs_0_, bf16[1,4096,256]{2,1,0:T(8,128)(2,1)S(1)} %get-tuple-element.9.refs_1_, ...), custom_call_target="tpu_custom_call" | custom-call | tf_op jit(solution)/shard_map/pallas_call | solution.py:472

commit v4 on v3

--- a/solution.py
+++ b/solution.py
@@ -46,6 +46,7 @@
     n_rows = n_fs * cap
     n_peer = n_z * n_x
     d_model = n_tp * wide
+    half = rows_g // 2
     sibling = (g, f, y * n_c + (1 - c))
 
     def remote(src, dst, s_sem, r_sem, to):
@@ -65,6 +66,30 @@
         zz = (z + off) % n_z
         xx = (x + 1 + i // n_z + turn) % n_x
         return zz // n_zl, (zz % n_zl) * n_x + xx
+
+    barrier = pltpu.get_barrier_semaphore()
+
+    def greet(i, carry):
+        pg, pf = peer(i)
+        pl.semaphore_signal(barrier, inc=1, device_id=(pg, pf, t), device_id_type=MESH)
+        return carry
+
+
+    def greet_down(i, carry):
+        to = (t // n_zl, (t % n_zl) * n_x + i // n_tp, i % n_tp)
+        mine = jnp.logical_and(z == t, jnp.logical_and(i // n_tp == x, i % n_tp == t))
+
+        @pl.when(jnp.logical_not(mine))
+        def _():
+            pl.semaphore_signal(barrier, inc=1, device_id=to, device_id_type=MESH)
+
+        return carry
+
+    lax.fori_loop(0, n_x * n_tp, greet_down, 0, unroll=True)
+    lax.fori_loop(0, n_peer - 1, greet, 0, unroll=True)
+    for dy in range(1, n_y):
+        pl.semaphore_signal(barrier, inc=1, device_id=(g, f, ((y + dy) % n_y) * n_c + c), device_id_type=MESH)
+    pl.semaphore_signal(barrier, inc=1, device_id=sibling, device_id_type=MESH)
 
     loads = [
         pltpu.make_async_copy(gate_hbm, stage_g, load_sem.at[0]),
@@ -79,30 +104,6 @@
     ]
     for copy in small + loads:
         copy.start()
-
-    barrier = pltpu.get_barrier_semaphore()
-
-    def greet(i, carry):
-        pg, pf = peer(i)
-        pl.semaphore_signal(barrier, inc=1, device_id=(pg, pf, t), device_id_type=MESH)
-        return carry
-
-    lax.fori_loop(0, n_peer - 1, greet, 0)
-
-    def greet_down(i, carry):
-        to = (t // n_zl, (t % n_zl) * n_x + i // n_tp, i % n_tp)
-        mine = jnp.logical_and(z == t, jnp.logical_and(i // n_tp == x, i % n_tp == t))
-
-        @pl.when(jnp.logical_not(mine))
-        def _():
-            pl.semaphore_signal(barrier, inc=1, device_id=to, device_id_type=MESH)
-
-        return carry
-
-    lax.fori_loop(0, n_x * n_tp, greet_down, 0)
-    for dy in range(1, n_y):
-        pl.semaphore_signal(barrier, inc=1, device_id=(g, f, ((y + dy) % n_y) * n_c + c), device_id_type=MESH)
-    pl.semaphore_signal(barrier, inc=1, device_id=sibling, device_id_type=MESH)
 
     for copy in small:
         copy.wait()
@@ -191,13 +192,16 @@
     lax.fori_loop(0, n_fs - 1, dispatch, 0)
 
     def send_gate(i, carry):
-        pg, pf = peer(i)
+        pg, pf = peer(i % (n_peer - 1))
+        first = pl.multiple_of(i // (n_peer - 1) * half, half)
         remote(
-            snd_g.at[pf], wg.at[pl.ds(pl.multiple_of(part * rows_g, rows_g), rows_g), :], w_s.at[0], g_r, (pg, pf, t)
+            snd_g.at[pf, pl.ds(first, half), :],
+            wg.at[pl.ds(pl.multiple_of(part * rows_g + first, half), half), :],
+            w_s.at[0], g_r, (pg, pf, t),
         ).start()
         return carry
 
-    lax.fori_loop(0, n_peer - 1, send_gate, 0)
+    lax.fori_loop(0, 2 * (n_peer - 1), send_gate, 0)
 
     wait_recv(xall.at[0, pl.ds(0, (n_fs - 1) * cap), :], disp_r)
     for dy in range(1, n_y):
@@ -205,13 +209,16 @@
     remote(xall.at[t], xall.at[t], sib_s, sib_r.at[0], sibling).start()
 
     def send_up(i, carry):
-        pg, pf = peer(i)
+        pg, pf = peer(i % (n_peer - 1))
+        first = pl.multiple_of(i // (n_peer - 1) * half, half)
         remote(
-            snd_u.at[pf], wu.at[pl.ds(pl.multiple_of(part * rows_g, rows_g), rows_g), :], w_s.at[1], u_r, (pg, pf, t)
+            snd_u.at[pf, pl.ds(first, half), :],
+            wu.at[pl.ds(pl.multiple_of(part * rows_g + first, half), half), :],
+            w_s.at[1], u_r, (pg, pf, t),
         ).start()
         return carry
 
-    lax.fori_loop(0, n_peer - 1, send_up, 0)
+    lax.fori_loop(0, 2 * (n_peer - 1), send_up, 0)
     for dy in range(1, n_y):
         from_tp = ((y + dy) % n_y) * n_c + c
         wait_recv(xall.at[from_tp], ag_r.at[dy])
@@ -406,8 +413,14 @@
 
 def write_out(*refs):
     n = len(refs) // 2
-    srcs, dsts, sem = refs[:n], refs[n : 2 * n], refs[2 * n]
-    copies = [pltpu.make_async_copy(src, dst, sem.at[i]) for i, (src, dst) in enumerate(zip(srcs, dsts))]
+    sem = refs[2 * n]
+    copies = []
+    for i, (src, dst) in enumerate(zip(refs[:n], refs[n : 2 * n])):
+        parts = 4 if len(src.shape) == 3 else 1
+        size = src.shape[-2] // parts
+        for p in range(parts):
+            rows = (slice(None),) * (len(src.shape) - 2) + (pl.ds(p * size, size),)
+            copies.append(pltpu.make_async_copy(src.at[rows], dst.at[rows], sem.at[i, p]))
     for copy in copies:
         copy.start()
     for copy in copies:
@@ -474,7 +487,7 @@
         out_shape=tuple(jax.ShapeDtypeStruct(r.shape, r.dtype) for r in results),
         in_specs=[vmem_spec] * 4,
         out_specs=(any_spec,) * 4,
-        scratch_shapes=[dma((4,))],
+        scratch_shapes=[dma((4, 4))],
         compiler_params=pltpu.CompilerParams(vmem_limit_bytes=1024 * 1024),
     )(*(pltpu.with_memory_space_constraint(r, pltpu.VMEM) for r in results))
 

time: 196 us -> 194 us (0.990)
  Pallas kernels: 195 us -> 192 us
    pallas_call x1, Pallas kernels: 193 us -> 189 us  [body(): pl.pallas_call(functools.partial(kernel, (n_gr, n_zl, n_x, n_y, n_c, cap)...]
where the time goes in v4:
time: 194 us; the launch traced here: 192 us
  Pallas kernels  192 us (99%)
    pallas_call x1, Pallas kernels, body(): pl.pallas_call(functools.partial(kernel, (n_gr, n_zl, n_x, n_y, n_c, cap)...  189 us

profile of v4, /device:TPU:32, one launch (start us, length us, event | category | flops | bytes accessed | tf_op | source)
XLA Modules:
  0.0 192.3 jit_solution(13194491360737320808)
XLA Ops:
  0.6 188.8 %shard_map.102 = (bf16[1,4096,256]{2,1,0:T(8,128)(2,1)S(1)}, bf16[1,4096,256]{2,1,0:T(8,128)(2,1)S(1)}, bf16[1,256,4096]{2,1,0:T(8,128)(2,1)S(1)}, bf16[192,512]{1,0:T(8,128)(2,1)S(1)}) custom-call(bf16[192,512]{1,0:T(8,128)(2,1)} %tok_hbm.1, s32[2,192]{1,0:T(2,128)} %bitcast.3, f32[2,192]{1,0:T(2,128)} %bitcast.4, f32[1,128]{1,0:T(1,128)} %bitcast.5, ...), custom_call_target="tpu_custom_call" | custom-call | tf_op jit(solution)/shard_map/pallas_call | solution.py:444
  189.5 2.8 %shard_map.103 = (bf16[1,4096,256]{2,1,0:T(8,128)(2,1)}, bf16[1,4096,256]{2,1,0:T(8,128)(2,1)}, bf16[1,256,4096]{2,1,0:T(8,128)(2,1)}, bf16[192,512]{1,0:T(8,128)(2,1)}) custom-call(bf16[1,4096,256]{2,1,0:T(8,128)(2,1)S(1)} %get-tuple-element.8.refs_0_, bf16[1,4096,256]{2,1,0:T(8,128)(2,1)S(1)} %get-tuple-element.9.refs_1_, ...), custom_call_target="tpu_custom_call" | custom-call | tf_op jit(solution)/shard_map/pallas_call | solution.py:485

commit v5 on v4

--- a/solution.py
+++ b/solution.py
@@ -346,6 +346,9 @@
         mixed_out[:, q * wq : (q + 1) * wq] = out.astype(BF16)
 
     for q in range(NQ):
+        if q == NQ - 1:
+            pass_chunk(q - 1)
+            finish(q - 2)
 
         @pl.when(z == t)
         def _(q=q):
@@ -382,15 +385,15 @@
             return carry
 
         lax.fori_loop(0, NR, exchange, 0)
-        if q > 0:
+        if 0 < q < NQ - 1:
             pass_chunk(q - 1)
-        if q > 1:
+        if 1 < q < NQ - 1:
             finish(q - 2)
         if q > 2:
             combine(q - 3)
+    finish(NQ - 2)
     pass_chunk(NQ - 1)
-    for q in range(max(NQ - 2, 0), NQ):
-        finish(q)
+    finish(NQ - 1)
     for q in range(max(NQ - 3, 0), NQ):
         combine(q)
 

time: 194 us -> 195 us (level); the launches traced: 192 us -> 195 us
  Pallas kernels: 192 us -> 195 us
    pallas_call x1, Pallas kernels: 189 us -> 192 us  [body(): pl.pallas_call(functools.partial(kernel, (n_gr, n_zl, n_x, n_y, n_c, cap)...]
where the time goes in v5:
time: 195 us
  Pallas kernels  195 us (100%)
    pallas_call x1, Pallas kernels, body(): pl.pallas_call(functools.partial(kernel, (n_gr, n_zl, n_x, n_y, n_c, cap)...  192 us

profile of v5, /device:TPU:32, one launch (start us, length us, event | category | flops | bytes accessed | tf_op | source)
XLA Modules:
  0.0 195.3 jit_solution(82601214074219107)
XLA Ops:
  0.6 191.9 %shard_map.102 = (bf16[1,4096,256]{2,1,0:T(8,128)(2,1)S(1)}, bf16[1,4096,256]{2,1,0:T(8,128)(2,1)S(1)}, bf16[1,256,4096]{2,1,0:T(8,128)(2,1)S(1)}, bf16[192,512]{1,0:T(8,128)(2,1)S(1)}) custom-call(bf16[192,512]{1,0:T(8,128)(2,1)} %tok_hbm.1, s32[2,192]{1,0:T(2,128)} %bitcast.3, f32[2,192]{1,0:T(2,128)} %bitcast.4, f32[1,128]{1,0:T(1,128)} %bitcast.5, ...), custom_call_target="tpu_custom_call" | custom-call | tf_op jit(solution)/shard_map/pallas_call | solution.py:447
  192.5 2.8 %shard_map.103 = (bf16[1,4096,256]{2,1,0:T(8,128)(2,1)}, bf16[1,4096,256]{2,1,0:T(8,128)(2,1)}, bf16[1,256,4096]{2,1,0:T(8,128)(2,1)}, bf16[192,512]{1,0:T(8,128)(2,1)}) custom-call(bf16[1,4096,256]{2,1,0:T(8,128)(2,1)S(1)} %get-tuple-element.8.refs_0_, bf16[1,4096,256]{2,1,0:T(8,128)(2,1)S(1)} %get-tuple-element.9.refs_1_, ...), custom_call_target="tpu_custom_call" | custom-call | tf_op jit(solution)/shard_map/pallas_call | solution.py:488
